TPU v7x, 256 devices: a whole 4x4x8 slice. The times are simulated.
256 devices in a mesh: fs: 16 (over y, x), tp: 16 (over z, core).
Axes of the slice: x: 4, y: 4, z: 8, core: 2. Of those that a mesh axis runs over, the one named last changes fastest.
Arguments:
- tokens: bfloat16 [16384, 2048], P(('fs', 'tp')), may hold values from -6 to 6
- gate_weight: bfloat16 [2048, 5632], P('fs', 'tp'), may hold values from -0.125 to 0.125
- up_weight: bfloat16 [2048, 5632], P('fs', 'tp'), may hold values from -0.125 to 0.125
- down_weight: bfloat16 [5632, 2048], P('tp', 'fs'), may hold values from -0.078125 to 0.078125
- grad_out: bfloat16 [16384, 2048], P(('fs', 'tp')), may hold values from -24 to 24
Outputs:
- grad_input: bfloat16 [16384, 2048], P(('fs', 'tp'))
- grad_gate: float32 [2048, 5632], P('fs', 'tp')
- grad_up: float32 [2048, 5632], P('fs', 'tp')
- grad_down: float32 [5632, 2048], P('tp', 'fs')
All inputs are finite; a program needn't handle non-finite values.
Results may differ from a plain program's by a relative error of at most 0.0049.
Values may be sent and summed in bfloat16 or wider, within the bound.
No kernel may reach another device: no remote copies, remote signals or barrier semaphores. Data moves between devices by JAX's collectives and lax.ppermute only.
A program may use at most 128 MiB of HBM per device.

v0:
```python
import jax
import jax.numpy as jnp
from jax import lax
from jax.sharding import PartitionSpec as P


def sent_together(arrays, axis, dim, along):
    widths = [a.shape[along] for a in arrays]
    both = jnp.concatenate(arrays, axis=along)
    whole = lax.all_gather(both, axis, axis=dim, tiled=True)
    return tuple(jnp.split(whole, [sum(widths[:k]) for k in range(1, len(widths))], axis=along))


def in_order(pieces, dim):
    dims = list(pieces.shape[1:])
    dims[dim] *= pieces.shape[0]
    return jnp.moveaxis(pieces, 0, dim).reshape(dims)


def copy_for_each(x, axis):
    length = lax.axis_size(axis)
    return lax.all_to_all(jnp.broadcast_to(x[None], (length, *x.shape)), axis, 0, 0, tiled=True)


def gather_directly(x, axis, dim):
    return in_order(copy_for_each(x, axis), dim)


def over_rows(left, right):
    return lax.dot_general(
        left, right, (((0,), (0,)), ((), ())), preferred_element_type=jnp.float32
    )


def over_cols(left, right):
    return lax.dot_general(
        left, right, (((1,), (1,)), ((), ())), preferred_element_type=jnp.float32
    )


def body(tokens, gate_weight, up_weight, down_weight, grad_out):
    tok_all, cot_all = sent_together((tokens, grad_out), "tp", 0, 1)
    gate_full, up_full = sent_together((gate_weight, up_weight), "fs", 0, 1)
    down_full = gather_directly(down_weight, "fs", 1)
    gate_pre = jnp.dot(tok_all, gate_full, preferred_element_type=jnp.float32)
    up_pre = jnp.dot(tok_all, up_full, preferred_element_type=jnp.float32)
    sig_gate = jax.nn.sigmoid(gate_pre)
    active = gate_pre * sig_gate
    hidden = (active * up_pre).astype(jnp.bfloat16)
    d_hidden = over_cols(cot_all, down_full)
    d_gate = (d_hidden * up_pre * sig_gate * (1.0 + gate_pre * (1.0 - sig_gate))).astype(
        jnp.bfloat16
    )
    d_up = (d_hidden * active).astype(jnp.bfloat16)
    grad_input = lax.psum_scatter(
        over_cols(d_gate, gate_full) + over_cols(d_up, up_full),
        "tp",
        scatter_dimension=0,
        tiled=True,
    ).astype(jnp.bfloat16)
    width = gate_full.shape[1]
    summed = lax.psum_scatter(
        jnp.concatenate(
            [over_rows(tok_all, d_gate), over_rows(tok_all, d_up), over_rows(cot_all, hidden)],
            axis=1,
        ),
        "fs",
        scatter_dimension=0,
        tiled=True,
    )
    grad_gate = summed[:, :width]
    grad_up = summed[:, width : 2 * width]
    grad_down = summed[:, 2 * width :].T
    return (grad_input, grad_gate, grad_up, grad_down)


def solution(mesh):
    in_specs = (
        P(("fs", "tp"), None),
        P("fs", "tp"),
        P("fs", "tp"),
        P("tp", "fs"),
        P(("fs", "tp"), None),
    )
    out_specs = (P(("fs", "tp"), None), P("fs", "tp"), P("fs", "tp"), P("tp", "fs"))
    return jax.shard_map(body, mesh=mesh, in_specs=in_specs, out_specs=out_specs, check_vma=False)
```

profile of v0, /device:TPU:4, one launch (start us, length us, event | category | flops | bytes accessed | tf_op | source)
XLA Modules:
  0.0 328.4 jit_solution(6695033487975725311)
XLA Ops:
  7.2 0.0 all-gather.5.cloned.1.call-start
  7.2 1.6 pad_maximum_fusion.2
  8.8 0.0 all-gather.5.cloned.1.call-update
  8.9 0.0 all-gather.3.cloned.1.call-start
  8.9 1.9 pad_maximum_fusion.1
  10.8 0.0 all-gather.3.cloned.1.call-update
  10.8 2.2 broadcast_in_dim.2
  13.0 7.4 %all-to-all-start = ((bf16[16,352,128]{2,1,0:T(8,128)(2,1)}), bf16[16,352,128]{2,1,0:T(8,128)(2,1)}, u32[]{:S(2)}, u32[]{:S(2)}) async-start(bf16[16,352,128]{2,1,0:T(8,128)(2,1)} %broadcast_in_dim.2), calls=%async_computation | async-start | bytes 2883584 | tf_op jit(solution)/shard_map/all_to_all | solution.py:22
  20.5 0.0 reduce-scatter.3.cloned.1.call-start
  20.5 55.7 %all-gather.5.cloned.1.call-done = bf16[2048,704]{0,1:T(8,128)(2,1)} async-done(((bf16[128,704]{0,1:T(8,128)(2,1)}), bf16[2048,704]{0,1:T(8,128)(2,1)}) %all-gather.5.cloned.1.call-update) | async-done | bytes 2883600 | tf_op jit(solution)/shard_map/all_gather | solution.py:10
  76.2 58.6 %all-gather.3.cloned.1.call-done = bf16[1024,4096]{1,0:T(8,128)(2,1)} async-done(((bf16[64,4096]{1,0:T(8,128)(2,1)}), bf16[1024,4096]{1,0:T(8,128)(2,1)}) %all-gather.3.cloned.1.call-update) | async-done | bytes 8388624 | tf_op jit(solution)/shard_map/all_gather | solution.py:10
  134.8 5.6 %fusion.8 = f32[1024,352]{0,1:T(8,128)} fusion(bf16[1024,4096]{1,0:T(8,128)(2,1)} %all-gather.3.cloned.1.call-done, bf16[2048,704]{0,1:T(8,128)(2,1)} %all-gather.5.cloned.1.call-done), kind=kOutput, calls=%fused_computation.10 | convolution fusion | flops 1476395008 | bytes 7077888 | tf_op jit(solution)/shard_map/dot_general | solution.py:45
  140.4 0.0 copy-done
  140.4 2.8 fusion.10
  143.2 0.0 all-to-all-done
  143.2 5.5 %multiply_convert_fusion.1 = (bf16[1024,352]{0,1:T(8,128)(2,1)S(1)}, bf16[1024,352]{0,1:T(8,128)(2,1)S(1)}) fusion(f32[1024,352]{0,1:T(8,128)} %fusion.8, f32[1024,352]{0,1:T(8,128)} %fusion.10, bf16[1024,4096]{1,0:T(8,128)(2,1)} %all-gather.3.cloned.1.call-done, bf16[16,352,128]{2,1,0:T(8,128)(2,1)} %all-to-all-done), kind=kOutput, calls=%fused_computation.17 | convolution fusion | flops 1481080832 | bytes 9961472 | tf_op jit(solution)/shard_map/dot_general | solution.py:36
  148.7 0.0 copy-start.3
  148.7 0.0 copy-start.1
  148.7 2.4 fusion.15
  151.2 5.9 %convolution_add_fusion = f32[1024,2048]{1,0:T(8,128)} fusion(f32[1024,2048]{1,0:T(8,128)S(1)} %fusion.15, bf16[1024,352]{0,1:T(8,128)(2,1)S(1)} %get-tuple-element.4, bf16[2048,704]{0,1:T(8,128)(2,1)S(1)} %copy-done), kind=kOutput, calls=%fused_computation.1 | convolution fusion | flops 1478492160 | bytes 18939904 | tf_op jit(solution)/shard_map/dot_general | solution.py:36
  157.0 0.0 reduce-scatter.3.cloned.1.call-update
  157.1 0.2 reduce-scatter.5.cloned.1.call-start
  157.3 0.8 copy-done.2
  158.1 3.8 %fusion.6 = f32[2048,352]{0,1:T(8,128)S(1)} fusion(bf16[1024,352]{0,1:T(8,128)(2,1)S(1)} %copy-done.2, bf16[1024,4096]{1,0:T(8,128)(2,1)} %all-gather.3.cloned.1.call-done), kind=kOutput, calls=%fused_computation.8 | convolution fusion | flops 1476395008 | bytes 7798784 | tf_op jit(solution)/shard_map/dot_general | solution.py:30
  162.0 4.0 %fusion.4 = f32[2048,352]{0,1:T(8,128)S(1)} fusion(bf16[1024,352]{0,1:T(8,128)(2,1)S(1)} %copy-done.4, bf16[1024,4096]{1,0:T(8,128)(2,1)} %all-gather.3.cloned.1.call-done), kind=kOutput, calls=%fused_computation.6 | convolution fusion | flops 1476395008 | bytes 7798784 | tf_op jit(solution)/shard_map/dot_general | solution.py:30
  166.0 4.3 %fusion = f32[2048,352]{0,1:T(8,128)S(1)} fusion(bf16[1024,4096]{1,0:T(8,128)(2,1)} %all-gather.3.cloned.1.call-done, f32[1024,352]{0,1:T(8,128)S(1)} %copy-done.7, f32[1024,352]{0,1:T(8,128)S(1)} %copy-done.6), kind=kOutput, calls=%fused_computation.2 | convolution fusion | flops 1478557696 | bytes 9961472 | tf_op jit(solution)/shard_map/dot_general | solution.py:30
  170.4 4.1 %pad_maximum_fusion = f32[2048,1056]{0,1:T(8,128)} fusion(f32[2048,352]{0,1:T(8,128)S(1)} %fusion, f32[2048,352]{0,1:T(8,128)S(1)} %fusion.6, f32[2048,352]{0,1:T(8,128)S(1)} %fusion.4), kind=kLoop, calls=%fused_computation | loop fusion | flops 4325376 | bytes 17301504 | tf_op jit(solution)/shard_map/concatenate | solution.py:63
  174.5 0.0 reduce-scatter.5.cloned.1.call-update
  174.5 51.9 %reduce-scatter.3.cloned.1.call-done = f32[64,2048]{1,0:T(8,128)} async-done(((f32[1024,2048]{1,0:T(8,128)}), f32[64,2048]{1,0:T(8,128)}) %reduce-scatter.3.cloned.1.call-update) | async-done | bytes 524304 | tf_op jit(solution)/shard_map/reduce_scatter | solution.py:55
  226.4 1.8 convert_element_type.14
  228.2 91.8 %reduce-scatter.5.cloned.1.call-done = f32[128,1056]{0,1:T(8,128)} async-done(((f32[2048,1056]{0,1:T(8,128)}), f32[128,1056]{0,1:T(8,128)}) %reduce-scatter.5.cloned.1.call-update) | async-done | bytes 540688 | tf_op jit(solution)/shard_map/reduce_scatter | solution.py:62
  320.0 1.9 slice_bitcast_fusion
  (12 shorter events, 0.0 us)
Async XLA Ops:
  7.2 69.0 %all-gather.5.cloned.1.call-start = ((), (), s32[]{:S(2)}) async-start(), calls=%async_computation.4 | async-start | bytes 3063808 | tf_op jit(solution)/shard_map/all_gather | solution.py:10
  8.9 125.9 %all-gather.3.cloned.1.call-start = ((), (), s32[]{:S(2)}) async-start(), calls=%async_computation.3 | async-start | bytes 8912896 | tf_op jit(solution)/shard_map/all_gather | solution.py:10
  13.0 130.2 %all-to-all-start = ((bf16[16,352,128]{2,1,0:T(8,128)(2,1)}), bf16[16,352,128]{2,1,0:T(8,128)(2,1)}, u32[]{:S(2)}, u32[]{:S(2)}) async-start(bf16[16,352,128]{2,1,0:T(8,128)(2,1)} %broadcast_in_dim.2), calls=%async_computation | async-start | bytes 2883584 | tf_op jit(solution)/shard_map/all_to_all | solution.py:22
  20.5 205.9 %reduce-scatter.3.cloned.1.call-start = ((), (), s32[]{:S(2)}) async-start(), calls=%async_computation.5 | async-start | bytes 8912896 | tf_op jit(solution)/shard_map/reduce_scatter | solution.py:55
  76.2 64.3 %copy-start = (bf16[2048,704]{0,1:T(8,128)(2,1)S(1)}, bf16[2048,704]{0,1:T(8,128)(2,1)}, u32[]{:S(2)}) copy-start(bf16[2048,704]{0,1:T(8,128)(2,1)} %all-gather.5.cloned.1.call-done) | copy-start | bytes 8650756
  134.8 5.6 %copy-start.5 = (bf16[1024,4096]{1,0:T(8,128)(2,1)S(1)}, bf16[1024,4096]{1,0:T(8,128)(2,1)}, u32[]{:S(2)}) copy-start(bf16[1024,4096]{1,0:T(8,128)(2,1)} %all-gather.3.cloned.1.call-done) | copy-start | bytes 25165828
  148.7 2.4 copy-start.3
  148.7 2.4 copy-start.1
  157.0 1.1 copy-start.2
  157.1 4.9 %copy-start.4 = (bf16[1024,352]{0,1:T(8,128)(2,1)S(1)}, bf16[1024,352]{0,1:T(8,128)(2,1)}, u32[]{:S(2)}) copy-start(bf16[1024,352]{0,1:T(8,128)(2,1)} %copy-done.3) | copy-start | bytes 2162692
  157.1 162.9 %reduce-scatter.5.cloned.1.call-start = ((), (), s32[]{:S(2)}) async-start(), calls=%async_computation.6 | async-start | bytes 9191424 | tf_op jit(solution)/shard_map/reduce_scatter | solution.py:62
  162.0 4.0 %copy-start.6 = (f32[1024,352]{0,1:T(8,128)S(1)}, f32[1024,352]{0,1:T(8,128)}, u32[]{:S(2)}) copy-start(f32[1024,352]{0,1:T(8,128)} %fusion.8) | copy-start | bytes 4325380
  162.0 4.0 %copy-start.7 = (f32[1024,352]{0,1:T(8,128)S(1)}, f32[1024,352]{0,1:T(8,128)}, u32[]{:S(2)}) copy-start(f32[1024,352]{0,1:T(8,128)} %fusion.10) | copy-start | bytes 4325380
Sparse Core Ops, SparseCore 0:
  11.0 65.1 all-gather.4
  78.0 56.7 all-gather.2
  157.2 69.1 reduce-scatter.2
  230.0 89.9 reduce-scatter.4
where the time goes:
time: 329 us; the launch traced here: 328 us
  waiting for transfers between devices  258 us (78%)
  matrix products  34.3 us (10%)
  between operations  13.9 us (4%)
  other arithmetic  9.42 us (3%)
  starting transfers between devices  7.79 us (2%)
  local copies, waits for them, and re-layouts  4.94 us (2%)
    all_gather x2, waiting for transfers between devices, sent_together(): whole = lax.all_gather(both, axis, axis=dim, tiled=True)  114 us
    reduce_scatter x1, waiting for transfers between devices, body(): lax.psum_scatter(jnp.concatenate([over_rows(tok_all, d_gate), over_rows(t...  91.8 us
    reduce_scatter x1, waiting for transfers between devices, body(): lax.psum_scatter(over_cols(d_gate, gate_full) + over_cols(d_up, up_full),...  51.9 us
    dot_general x3, matrix products, over_cols(): lax.dot_general(left, right, (((1,), (1,)), ((), ())), preferred_element_...  13.7 us
    dot_general x3, matrix products, over_rows(): lax.dot_general(left, right, (((0,), (0,)), ((), ())), preferred_element_...  12.2 us
    all_to_all x1, starting transfers between devices, copy_for_each(): lax.all_to_all(jnp.broadcast_to(x[None], (length, *x.shape)), axis, 0, 0,...  7.45 us
  transfers between devices with their start and end apart: 5, of which 4 were waited for; matrix products, arithmetic and copies ran while one was open for 9% of the time, Pallas kernels for 0%

commit v1 on v0

v1 whole, which is shorter than its diff:
```python
import functools

import jax
import jax.numpy as jnp
from jax import lax
from jax.experimental import pallas as pl
from jax.experimental.pallas import tpu as pltpu
from jax.sharding import Mesh
from jax.sharding import PartitionSpec as P


OFFSET = (0, 1, 3, 2)
SIZES = {"y": 4, "x": 4, "z": 8, "core": 2}
BF = jnp.bfloat16
F32 = jnp.float32
VMEM = pl.BlockSpec(memory_space=pltpu.VMEM)
SMEM = pl.BlockSpec(memory_space=pltpu.SMEM)


def shift(a, axis, by):
    n = SIZES[axis]
    return lax.ppermute(a, axis, [(i, (i + by) % n) for i in range(n)])


def shift_plane(a, first, by):
    pairs = []
    for y in range(4):
        for x in range(4):
            for core in range(2):
                along_x = (core == 0) == first
                to_y, to_x = (y, (x + by) % 4) if along_x else ((y + by) % 4, x)
                pairs.append(((y * 4 + x) * 2 + core, (to_y * 4 + to_x) * 2 + core))
    return lax.ppermute(a, ("y", "x", "core"), pairs)


def dot(left, right, dims):
    return lax.dot_general(left, right, (dims, ((), ())), preferred_element_type=F32)


def place(idx, p, s):
    y, x, core = idx[0], idx[1], idx[2]
    p, s = p ^ (p >> 1), s ^ (s >> 1)
    dy, dx = jnp.where(core == 0, s, p), jnp.where(core == 0, p, s)
    return pl.multiple_of((((y + dy) & 3) * 4 + ((x + dx) & 3)) * 128, 128)


def back_kernel(idx, own, right, left, out):
    for k in range(16):
        c = slice(k * 128, (k + 1) * 128)
        total = own[:, c] + right[:, c].astype(F32) + left[:, c].astype(F32)
        out[:, pl.ds(place(idx, k // 4, k % 4), 128)] = total.astype(BF)


def turn_back(idx, own, right, left):
    return pl.pallas_call(
        back_kernel,
        out_shape=jax.ShapeDtypeStruct(own.shape, BF),
        in_specs=[SMEM, VMEM, VMEM, VMEM],
        out_specs=VMEM,
        compiler_params=pltpu.CompilerParams(vmem_limit_bytes=8 * 2**20),
        name="turn_back",
    )(idx, own, right, left)


def call(kernel, outs, ins, scratch=(), limit=8, scalars=0):
    return pl.pallas_call(
        kernel,
        out_shape=tuple(jax.ShapeDtypeStruct(shape, dtype) for shape, dtype in outs),
        in_specs=[SMEM] * scalars + [VMEM] * (len(ins) - scalars),
        out_specs=(VMEM,) * len(outs),
        scratch_shapes=[pltpu.VMEM(shape, dtype) for shape, dtype in scratch],
        compiler_params=pltpu.CompilerParams(vmem_limit_bytes=limit * 2**20),
    )(*ins)


def lanes(k, n=128):
    return slice(k * n, (k + 1) * n)


def assemble_kernel(*refs):
    first, mine, send = refs[:3], refs[3], refs[4]
    n = mine.shape[0]

    def step(s, carry):
        for p in range(3):
            block = first[p][pl.ds(pl.multiple_of(s * n, 32), n)]
            mine[:, pl.ds(pl.multiple_of(s * 128 + p * 512, 128), 128)] = block
            send[:, pl.ds(pl.multiple_of(s * 384 + p * 128, 128), 128)] = block
        return carry

    lax.fori_loop(0, 4, step, 0)


def last_kernel(up, down, mine):
    n = mine.shape[0]
    for s in range(4):
        mine[:, lanes(s)] = (up if s < 2 else down)[(s % 2) * n : (s % 2 + 1) * n]


def weights_of(refs, rows, core):
    return jnp.concatenate([ref[rows] for ref in refs[2 * core : 2 * core + 2]], 1)


def theirs_order(a):
    most = [a[:, s * 512 : s * 512 + 384] for s in range(4)]
    return jnp.concatenate(most + [a[:, s * 512 + 384 : (s + 1) * 512] for s in range(4)], 1)


def forward_kernel(idx, *refs):
    blocks, w, (held, *outs) = refs[:16], refs[16:20], refs[20:]

    def turn(k, carry):
        at = pl.ds(place(idx, k >> 2, k & 3), 128)
        to = pl.ds(pl.multiple_of(k * 128, 128), 128)
        for m in range(16):
            held[m * 64 : m * 64 + 64, to] = blocks[m][:, at]
        return carry

    lax.fori_loop(0, 16, turn, 0)
    h = w[0].shape[0] // 3

    def half(n, carry):
        to = pl.ds(pl.multiple_of(n * 256, 256), 256)
        tok, cot = held[to], held[pl.ds(pl.multiple_of(512 + n * 256, 256), 256)]
        for core in range(2):
            d_pre, hid = outs[core], outs[core + 2]
            if core:
                tok, cot = theirs_order(tok), theirs_order(cot)
            pre = dot(weights_of(w, slice(0, 2 * h), core), tok, ((1,), (1,)))
            d_hidden = dot(weights_of(w, slice(2 * h, 3 * h), core), cot, ((1,), (1,)))
            gate_pre, up_pre = pre[:h], pre[h:]
            sig = jax.nn.sigmoid(gate_pre)
            active = gate_pre * sig
            hid[:, to] = (active * up_pre).astype(BF)
            d_pre[:h, to] = (d_hidden * up_pre * sig * (1.0 + gate_pre * (1.0 - sig))).astype(BF)
            d_pre[h:, to] = (d_hidden * active).astype(BF)
        return carry

    lax.fori_loop(0, 2, half, 0)


def forward(idx, toks, cots, w):
    d, h = 2048, w[0].shape[0] // 3
    outs = [((1024, d), BF)] + [((2 * h, 512), BF)] * 2 + [((h, 512), BF)] * 2
    return call(forward_kernel, outs, (idx, *toks, *cots, *w), limit=16, scalars=1)


def input_kernel(d_mine, d_other, m_most, m_last, o_most, o_last, *refs, half):
    outs, (a, b) = refs[:-2], refs[-2:]
    a[...] = d_mine[:, lanes(half, 256)].T
    b[...] = d_other[:, lanes(half, 256)].T
    n = d_mine.shape[0]

    def cols(start, width=256):
        return pl.ds(pl.multiple_of(start, 128), width)

    def one(p, k, mine):
        if k:
            other = jnp.concatenate([o_most[:n, cols(p * 384 + 256, 128)], o_last[:n, cols(p * 128, 128)]], 1)
        else:
            other = o_most[:n, cols(p * 384)]
        part = dot(a[...], mine, ((1,), (0,))) + dot(b[...], other, ((1,), (0,)))
        for m, out in enumerate(outs):
            out[:, cols(p * 512 + k * 256)] = part[m * 64 : m * 64 + 64].astype(out.dtype)

    def step(p, carry):
        for k in range(2):
            one(p, k, m_most[:n, cols(p * 512 + k * 256)])
        return carry

    lax.fori_loop(0, 3, step, 0)
    for k in range(2):
        one(3, k, m_last[:n, lanes(k, 256)])


def to_input(d_mine, d_other, w, half, types):
    d, n = 2048, d_mine.shape[0]
    outs = [((64, d), dtype) for dtype in types]
    kernel = functools.partial(input_kernel, half=half)
    return call(kernel, outs, (d_mine, d_other, *w), [((256, n), BF)] * 2, 16)


def grads_at(at, d, h, held):
    dims = ((1,), (0,))
    cols = lambda rows: jnp.concatenate([held[rows, c] for c in at], 1)
    return dot(d[...], cols(slice(0, 512)), dims), dot(h[...], cols(slice(512, 1024)), dims)


def theirs_kernel(d, h, held, out, *, pair):
    n = d.shape[0]

    def step(k, carry):
        at = [pl.ds(pl.multiple_of(k * 1024 + s * 512 + pair * 128, 128), 256) for s in range(2)]
        top, low = grads_at(at, d, h, held)
        for m in range(2):
            for s in range(2):
                to, of = pl.ds(pl.multiple_of(m * 512 + k * 256 + s * 128, 128), 128), lanes(2 * s + m)
                out[:n, to] = top[:, of].astype(BF)
                out[n:, to] = low[:, of].astype(BF)
        return carry

    if pair:
        for k in range(2):
            step(k, 0)
    else:
        lax.fori_loop(0, 2, step, 0)


def own_kernel(d, h, held, theirs, *outs, pair):
    n = d.shape[0]

    for m in range(2):

        def step(k, carry, m=m, width=512 if pair else 256):
            col = lambda base: pl.ds(pl.multiple_of(base + k * width, 256), width)
            top, low = grads_at([col((pair + m) * 512)], d, h, held)
            outs[m][:n, col(0)] = (top + theirs[:n, col(m * 512)].astype(F32)).astype(outs[m].dtype)
            outs[m][n:, col(0)] = (low + theirs[n:, col(m * 512)].astype(F32)).astype(outs[m].dtype)
            return carry

        lax.fori_loop(0, 1 if pair else 2, step, 0)


def theirs_grads(ins, pair):
    n = ins[0].shape[0] + ins[1].shape[0]
    return call(functools.partial(theirs_kernel, pair=pair), [((n, 1024), BF)], ins, limit=16)[0]


def own_grads(ins, theirs, pair):
    n = ins[0].shape[0] + ins[1].shape[0]
    outs = [((n, 512), F32 if pair + m == 0 else BF) for m in range(2)]
    return call(functools.partial(own_kernel, pair=pair), outs, (*ins, theirs), limit=20)


def sum_kernel(own, r1, r2, r3, keep, *outs):
    def step(k, carry):
        rows = pl.ds(pl.multiple_of(k * 352, 32), 352)
        total = own[rows] + (r1[rows].astype(F32) + r2[rows].astype(F32)) + r3[rows].astype(F32)
        keep[rows] = total[:, :128]
        for s, out in enumerate(outs):
            out[rows] = total[:, lanes(s + 1)].astype(BF)
        return carry

    lax.fori_loop(0, 3, step, 0)


def add_kernel(own, got, out):
    out[...] = (own[...] + got[...].astype(F32)).astype(BF)


def add(own, got):
    return call(add_kernel, [(own.shape, BF)], (own, got))[0]


def spread(a, first):
    return [a] + [shift_plane(a, first, -OFFSET[q]) for q in (1, 2, 3)]


def inner(tokens, gate_weight, up_weight, down_weight, grad_out):
    idx = jnp.stack([lax.axis_index(a) for a in ("y", "x", "core")]).astype(jnp.int32)
    h = gate_weight.shape[1]
    w = jnp.concatenate([gate_weight.T, up_weight.T, down_weight], 0)
    n = w.shape[0]
    ring = jnp.concatenate(spread(w, False), 0)
    up, down = shift_plane(ring, True, -1), shift_plane(ring, True, 1)
    m_most, send = call(assemble_kernel, [((n, 1536), BF)] * 2, (ring, up, down))
    up, down = shift_plane(up[: 2 * n], True, -1), shift_plane(down[2 * n :], True, 1)
    (m_last,) = call(last_kernel, [((n, 512), BF)], (up, down))
    weights = (m_most, m_last, shift(send, "core", 1), shift(m_last, "core", 1))

    toks, cots = {0: tokens}, {0: grad_out}
    for k in range(1, 4):
        for held in (toks, cots):
            held[k] = shift(held[k - 1], "z", -1)
            held[-k] = shift(held[1 - k], "z", 1)
    toks[4], cots[4] = shift(toks[3], "z", -1), shift(cots[-3], "z", 1)

    ring = (0, 1, -1, 2, -2, 3, -3, 4)
    held, dm, do, hm, ho = forward(idx, [toks[k] for k in ring], [cots[k] for k in ring], weights)
    far = to_input(dm, do, weights, 1, [F32] * 2 + [BF] * 2)
    gi = dict(zip(ring, [*to_input(dm, do, weights, 0, [F32] * 4), *far]))

    m_r, m_l = add(gi[3], shift(gi[4], "z", 1)), gi[-3]
    for k in (2, 1):
        m_r, m_l = shift(m_r, "z", 1), shift(m_l, "z", -1)
        m_r, m_l = add(gi[k], m_r), add(gi[-k], m_l)
    m_r, m_l = shift(m_r, "z", 1), shift(m_l, "z", -1)
    grad_input = turn_back(idx, gi[0], m_r, m_l)

    theirs_ins = (do, ho, held)
    own_ins = (dm, hm, held)
    sent = [theirs_grads(theirs_ins, pair) for pair in (2, 0)]
    got = [shift(a, "core", 1) for a in sent]
    (p2, p3), (p0, p1) = (own_grads(own_ins, a, pair) for a, pair in zip(got, (2, 0)))
    r = [shift_plane(a, True, OFFSET[q]) for q, a in ((1, p1), (2, p2), (3, p3))]
    keep, *sends = call(sum_kernel, [((n, 128), F32)] + [((n, 128), BF)] * 3, (p0, *r), limit=4)
    r = [shift_plane(a, False, OFFSET[q + 1]) for q, a in enumerate(sends)]
    grads = keep + (r[0].astype(F32) + r[1].astype(F32)) + r[2].astype(F32)
    return grad_input, grads[:h].T, grads[h : 2 * h].T, grads[2 * h :]


def solution(mesh):
    fine = Mesh(mesh.devices.reshape(4, 4, 8, 2), ("y", "x", "z", "core"))
    fs, tp = ("y", "x"), ("z", "core")
    rows = P(fs + tp, None)
    in_specs = (rows, P(fs, tp), P(fs, tp), P(tp, fs), rows)
    out_specs = (rows, P(fs, tp), P(fs, tp), P(tp, fs))
    return jax.shard_map(inner, mesh=fine, in_specs=in_specs, out_specs=out_specs, check_vma=False)
```

time: 329 us -> 168 us (0.51)
  waiting for transfers between devices: 258 us -> 59.7 us
  starting transfers between devices: 7.79 us -> 55.3 us
  matrix products: 34.3 us -> 0 us
  Pallas kernels: 0 us -> 31.9 us
  between operations: 13.9 us -> 0.92 us
  local copies, waits for them, and re-layouts: 4.94 us -> 17.9 us
  other arithmetic: 9.42 us -> 1.19 us
    reduce_scatter x2 -> x0, waiting for transfers between devices: 144 us -> none  [the longest x1 91.8 us: body(): lax.psum_scatter(jnp.concatenate([over_rows(tok_all, d_gate), over_rows(t...]
    all_gather x2 -> x0, waiting for transfers between devices: 114 us -> none  [sent_together(): whole = lax.all_gather(both, axis, axis=dim, tiled=True)]
    ppermute x0 -> x38, waiting for transfers between devices: none -> 59.7 us  [the longest x25 38.8 us: shift(): return lax.ppermute(a, axis, [(i, (i + by) % n) for i in range(n)])]
    ppermute x0 -> x38, starting transfers between devices: none -> 55.3 us  [the longest x25 32.8 us: shift(): return lax.ppermute(a, axis, [(i, (i + by) % n) for i in range(n)])]
    dot_general x8 -> x0, matrix products: 34.3 us -> none  [the longest x3 13.7 us: over_cols(): lax.dot_general(left, right, (((1,), (1,)), ((), ())), preferred_element_...]
    pallas_call x0 -> x16, Pallas kernels: none -> 31.9 us  [the longest x15 30.6 us: call(): pl.pallas_call(kernel, out_shape=tuple((jax.ShapeDtypeStruct(shape, dtype...]
    unnamed x16 -> x43, local copies, waits for them, and re-layouts: 0.87 us -> 17 us
    all_to_all x1 -> x0, starting transfers between devices: 7.45 us -> none  [copy_for_each(): lax.all_to_all(jnp.broadcast_to(x[None], (length, *x.shape)), axis, 0, 0,...]
  transfers between devices with their start and end apart: 5 -> 38, of which waited for: 4 -> 21; matrix products, arithmetic and copies ran while one was open for 9% -> 2% of each run, Pallas kernels for 0% -> 11%
where the time goes in v1:
time: 168 us; the launch traced here: 167 us
  waiting for transfers between devices  59.7 us (36%)
  starting transfers between devices  55.3 us (33%)
  Pallas kernels  31.9 us (19%)
  local copies, waits for them, and re-layouts  17.9 us (11%)
    ppermute x25, waiting for transfers between devices, shift(): return lax.ppermute(a, axis, [(i, (i + by) % n) for i in range(n)])  38.8 us
    ppermute x25, starting transfers between devices, shift(): return lax.ppermute(a, axis, [(i, (i + by) % n) for i in range(n)])  32.8 us
    pallas_call x15, Pallas kernels, call(): pl.pallas_call(kernel, out_shape=tuple((jax.ShapeDtypeStruct(shape, dtype...  30.6 us
    ppermute x13, starting transfers between devices, shift_plane(): return lax.ppermute(a, ('y', 'x', 'core'), pairs)  22.5 us
    ppermute x13, waiting for transfers between devices, shift_plane(): return lax.ppermute(a, ('y', 'x', 'core'), pairs)  20.9 us
    unnamed x43, local copies, waits for them, and re-layouts  17 us
  transfers between devices with their start and end apart: 38, of which 21 were waited for; matrix products, arithmetic and copies ran while one was open for 2% of the time, Pallas kernels for 11%

profile of v1, /device:TPU:4, one launch (start us, length us, event | category | flops | bytes accessed | tf_op | source)
XLA Modules:
  0.0 167.0 jit_solution(16255700178648841157)
XLA Ops:
  1.6 3.3 %collective-permute-start.16 = (bf16[1056,128]{1,0:T(8,128)(2,1)S(1)}, bf16[1056,128]{1,0:T(8,128)(2,1)S(1)}, u32[]{:S(2)}, u32[]{:S(2)}) collective-permute-start(bf16[1056,128]{1,0:T(8,128)(2,1)S(1)} %pad_maximum_fusion), channel_id=1, source_target_pairs={{0,128},{1,33},{16,144},{17,49},{32,160},{33,1},{48,176},{49,17},{... | collective-permute-start | bytes 811016 | tf_op jit(solution)/shard_map/ppermute | solution.py:33
  5.6 2.6 %collective-permute-start.14 = (bf16[1056,128]{1,0:T(8,128)(2,1)S(1)}, bf16[1056,128]{1,0:T(8,128)(2,1)S(1)}, u32[]{:S(2)}, u32[]{:S(2)}) collective-permute-start(bf16[1056,128]{1,0:T(8,128)(2,1)S(1)} %pad_maximum_fusion), channel_id=1, source_target_pairs={{0,192},{1,49},{16,208},{17,1},{32,224},{33,17},{48,240},{49,33},{... | collective-permute-start | bytes 811016 | tf_op jit(solution)/shard_map/ppermute | solution.py:33
  10.9 2.1 %collective-permute-done.14 = bf16[1056,128]{1,0:T(8,128)(2,1)S(1)} collective-permute-done((bf16[1056,128]{1,0:T(8,128)(2,1)S(1)}, bf16[1056,128]{1,0:T(8,128)(2,1)S(1)}, u32[]{:S(2)}, u32[]{:S(2)}) %collective-permute-start.14) | collective-permute-done | bytes 270368 | tf_op jit(solution)/shard_map/ppermute | solution.py:33
  15.2 13.1 %collective-permute-done.18.refs_2_ = bf16[4224,128]{1,0:T(8,128)(2,1)S(1)} collective-permute-done((bf16[4224,128]{1,0:T(8,128)(2,1)S(1)}, bf16[4224,128]{1,0:T(8,128)(2,1)S(1)}, u32[]{:S(2)}, u32[]{:S(2)}) %collective-permute-start.18) | collective-permute-done | bytes 1081376 | tf_op jit(solution)/shard_map/ppermute | solution.py:33
  29.5 2.7 %shard_map.84 = (bf16[1056,1536]{1,0:T(8,128)(2,1)S(1)}, bf16[1056,1536]{1,0:T(8,128)(2,1)}) custom-call(bf16[4224,128]{1,0:T(8,128)(2,1)S(1)} %constant_dynamic-update-slice_fusion.refs_0_, bf16[4224,128]{1,0:T(8,128)(2,1)S(1)} %collective-permute-done.17.refs_1_, bf16[4224,128]{1,0:T(8,128)(2,1)S(1)} %collective-permute-done.18.refs_2_), custom_call_target="tpu_custom_call" | custom-call | tf_op jit(solution)/shard_map/pallas_call | solution.py:66
  32.2 3.1 %collective-permute-start.20 = (bf16[2112,128]{1,0:T(8,128)(2,1)S(1)}, bf16[2112,128]{1,0:T(8,128)(2,1)S(1)}, u32[]{:S(2)}, u32[]{:S(2)}) collective-permute-start(bf16[2112,128]{1,0:T(8,128)(2,1)S(1)} %slice.21), channel_id=1, source_target_pairs={{0,16},{1,65},{16,32},{17,81},{32,48},{33,97},{48,0},{49,113},{64,... | collective-permute-start | bytes 1622024 | tf_op jit(solution)/shard_map/ppermute | solution.py:33
  35.4 4.9 %collective-permute-start = (bf16[64,2048]{1,0:T(8,128)(2,1)S(1)}, bf16[64,2048]{1,0:T(8,128)(2,1)S(1)}, u32[]{:S(2)}, u32[]{:S(2)}) collective-permute-start(bf16[64,2048]{1,0:T(8,128)(2,1)S(1)} %copy-done), channel_id=1, source_target_pairs={{0,14},{2,0},{4,2},{6,4},{8,6},{10,8},{12,10},{14,12},{1,15},{3,1}... | collective-permute-start | bytes 786440 | tf_op jit(solution)/shard_map/ppermute | solution.py:22
  42.2 2.6 %collective-permute-done.19.up = bf16[2112,128]{1,0:T(8,128)(2,1)S(1)} collective-permute-done((bf16[2112,128]{1,0:T(8,128)(2,1)S(1)}, bf16[2112,128]{1,0:T(8,128)(2,1)S(1)}, u32[]{:S(2)}, u32[]{:S(2)}) %collective-permute-start.19) | collective-permute-done | bytes 540704 | tf_op jit(solution)/shard_map/ppermute | solution.py:33
  46.0 4.5 %collective-permute-start.7 = (bf16[64,2048]{1,0:T(8,128)(2,1)S(1)}, bf16[64,2048]{1,0:T(8,128)(2,1)S(1)}, u32[]{:S(2)}, u32[]{:S(2)}) collective-permute-start(bf16[64,2048]{1,0:T(8,128)(2,1)S(1)} %copy-done.1), channel_id=1, source_target_pairs={{0,14},{2,0},{4,2},{6,4},{8,6},{10,8},{12,10},{14,12},{1,15},{3,1}... | collective-permute-start | bytes 786440 | tf_op jit(solution)/shard_map/ppermute | solution.py:22
  50.6 3.2 %collective-permute-start.2 = (bf16[64,2048]{1,0:T(8,128)(2,1)S(1)}, bf16[64,2048]{1,0:T(8,128)(2,1)S(1)}, u32[]{:S(2)}, u32[]{:S(2)}) collective-permute-start(bf16[64,2048]{1,0:T(8,128)(2,1)S(1)} %collective-permute-done.refs_1_), channel_id=1, source_target_pairs={{0,14},{2,0},{4,2},{6,4},{8,6},{10,8},{12,10},{14,12},{1,15},{3,1}... | collective-permute-start | bytes 786440 | tf_op jit(solution)/shard_map/ppermute | solution.py:22
  54.5 2.8 %collective-permute-done.7.refs_9_ = bf16[64,2048]{1,0:T(8,128)(2,1)S(1)} collective-permute-done((bf16[64,2048]{1,0:T(8,128)(2,1)S(1)}, bf16[64,2048]{1,0:T(8,128)(2,1)S(1)}, u32[]{:S(2)}, u32[]{:S(2)}) %collective-permute-start.7) | collective-permute-done | bytes 262176 | tf_op jit(solution)/shard_map/ppermute | solution.py:22
  58.0 2.2 %collective-permute-done.8.refs_10_ = bf16[64,2048]{1,0:T(8,128)(2,1)S(1)} collective-permute-done((bf16[64,2048]{1,0:T(8,128)(2,1)S(1)}, bf16[64,2048]{1,0:T(8,128)(2,1)S(1)}, u32[]{:S(2)}, u32[]{:S(2)}) %collective-permute-start.8) | collective-permute-done | bytes 262176 | tf_op jit(solution)/shard_map/ppermute | solution.py:22
  63.6 3.0 %collective-permute-done.3.refs_4_ = bf16[64,2048]{1,0:T(8,128)(2,1)S(1)} collective-permute-done((bf16[64,2048]{1,0:T(8,128)(2,1)S(1)}, bf16[64,2048]{1,0:T(8,128)(2,1)S(1)}, u32[]{:S(2)}, u32[]{:S(2)}) %collective-permute-start.3) | collective-permute-done | bytes 262176 | tf_op jit(solution)/shard_map/ppermute | solution.py:22
  70.0 2.2 %collective-permute-done.10.refs_12_ = bf16[64,2048]{1,0:T(8,128)(2,1)S(1)} collective-permute-done((bf16[64,2048]{1,0:T(8,128)(2,1)S(1)}, bf16[64,2048]{1,0:T(8,128)(2,1)S(1)}, u32[]{:S(2)}, u32[]{:S(2)}) %collective-permute-start.10) | collective-permute-done | bytes 262176 | tf_op jit(solution)/shard_map/ppermute | solution.py:22
  73.6 3.8 %collective-permute-start.11 = (bf16[64,2048]{1,0:T(8,128)(2,1)}, bf16[64,2048]{1,0:T(8,128)(2,1)}, u32[]{:S(2)}, u32[]{:S(2)}) collective-permute-start(bf16[64,2048]{1,0:T(8,128)(2,1)} %collective-permute-done.9.refs_11_), channel_id=1, source_target_pairs={{0,14},{2,0},{4,2},{6,4},{8,6},{10,8},{12,10},{14,12},{1,15},{3,1}... | collective-permute-start | bytes 786440 | tf_op jit(solution)/shard_map/ppermute | solution.py:22
  77.4 2.0 %collective-permute-done.5.refs_6_ = bf16[64,2048]{1,0:T(8,128)(2,1)S(1)} collective-permute-done((bf16[64,2048]{1,0:T(8,128)(2,1)S(1)}, bf16[64,2048]{1,0:T(8,128)(2,1)S(1)}, u32[]{:S(2)}, u32[]{:S(2)}) %collective-permute-start.5) | collective-permute-done | bytes 262176 | tf_op jit(solution)/shard_map/ppermute | solution.py:22
  80.1 2.0 %collective-permute-start.6 = (bf16[64,2048]{1,0:T(8,128)(2,1)}, bf16[64,2048]{1,0:T(8,128)(2,1)}, u32[]{:S(2)}, u32[]{:S(2)}) collective-permute-start(bf16[64,2048]{1,0:T(8,128)(2,1)} %collective-permute-done.4.refs_5_), channel_id=1, source_target_pairs={{0,14},{2,0},{4,2},{6,4},{8,6},{10,8},{12,10},{14,12},{1,15},{3,1}... | collective-permute-start | bytes 786440 | tf_op jit(solution)/shard_map/ppermute | solution.py:22
  84.4 3.4 %collective-permute-done.6.refs_7_ = bf16[64,2048]{1,0:T(8,128)(2,1)} collective-permute-done((bf16[64,2048]{1,0:T(8,128)(2,1)}, bf16[64,2048]{1,0:T(8,128)(2,1)}, u32[]{:S(2)}, u32[]{:S(2)}) %collective-permute-start.6) | collective-permute-done | bytes 262176 | tf_op jit(solution)/shard_map/ppermute | solution.py:22
  87.8 4.2 %collective-permute-done.13.refs_15_ = bf16[64,2048]{1,0:T(8,128)(2,1)} collective-permute-done((bf16[64,2048]{1,0:T(8,128)(2,1)}, bf16[64,2048]{1,0:T(8,128)(2,1)}, u32[]{:S(2)}, u32[]{:S(2)}) %collective-permute-start.13) | collective-permute-done | bytes 262176 | tf_op jit(solution)/shard_map/ppermute | solution.py:22
  100.6 9.3 %shard_map.86 = (bf16[1024,2048]{1,0:T(8,128)(2,1)S(1)}, bf16[704,512]{1,0:T(8,128)(2,1)S(1)}, bf16[704,512]{1,0:T(8,128)(2,1)S(1)}, bf16[352,512]{1,0:T(8,128)(2,1)S(1)}, bf16[352,512]{1,0:T(8,128)(2,1)S(1)}) custom-call(s32[3]{0:T(128)S(1)} %pad_add_fusion.idx, bf16[64,2048]{1,0:T(8,128)(2,1)S(1)} %copy-done, bf16[64,2048]{1,0:T(8,128)(2,1)S(1)} %copy-done.4, ...), custom_call_target="tpu_custom_call" | custom-call | tf_op jit(solution)/shard_map/pallas_call | solution.py:66
  113.8 2.4 %collective-permute-done.30.theirs = bf16[1056,1024]{1,0:T(8,128)(2,1)S(1)} collective-permute-done((bf16[1056,1024]{1,0:T(8,128)(2,1)S(1)}, bf16[1056,1024]{1,0:T(8,128)(2,1)S(1)}, u32[]{:S(2)}, u32[]{:S(2)}) %collective-permute-start.30) | collective-permute-done | bytes 2162720 | tf_op jit(solution)/shard_map/ppermute | solution.py:22
  121.7 2.5 %collective-permute-start.34 = (bf16[1056,512]{1,0:T(8,128)(2,1)S(1)}, bf16[1056,512]{1,0:T(8,128)(2,1)S(1)}, u32[]{:S(2)}, u32[]{:S(2)}) collective-permute-start(bf16[1056,512]{1,0:T(8,128)(2,1)S(1)} %get-tuple-element.45), channel_id=1, source_target_pairs={{0,32},{1,129},{16,48},{17,145},{32,0},{33,161},{48,16},{49,177},{... | collective-permute-start | bytes 3244040 | tf_op jit(solution)/shard_map/ppermute | solution.py:33
  124.2 5.1 %shard_map.88 = (f32[64,2048]{1,0:T(8,128)S(1)}, f32[64,2048]{1,0:T(8,128)S(1)}, bf16[64,2048]{1,0:T(8,128)(2,1)S(1)}, bf16[64,2048]{1,0:T(8,128)(2,1)S(1)}) custom-call(bf16[704,512]{1,0:T(8,128)(2,1)S(1)} %get-tuple-element.29.d_mine.d, bf16[704,512]{1,0:T(8,128)(2,1)S(1)} %get-tuple-element.30.d_other.d, ...), custom_call_target="tpu_custom_call" | custom-call | tf_op jit(solution)/shard_map/pallas_call | solution.py:66
  129.4 3.2 %collective-permute-start.27 = (bf16[64,2048]{1,0:T(8,128)(2,1)S(1)}, bf16[64,2048]{1,0:T(8,128)(2,1)S(1)}, u32[]{:S(2)}, u32[]{:S(2)}) collective-permute-start(bf16[64,2048]{1,0:T(8,128)(2,1)S(1)} %get-tuple-element.38), channel_id=1, source_target_pairs={{0,14},{2,0},{4,2},{6,4},{8,6},{10,8},{12,10},{14,12},{1,15},{3,1}... | collective-permute-start | bytes 786440 | tf_op jit(solution)/shard_map/ppermute | solution.py:22
  132.6 5.8 %collective-permute-done.23.got = bf16[64,2048]{1,0:T(8,128)(2,1)S(1)} collective-permute-done((bf16[64,2048]{1,0:T(8,128)(2,1)S(1)}, bf16[64,2048]{1,0:T(8,128)(2,1)S(1)}, u32[]{:S(2)}, u32[]{:S(2)}) %collective-permute-start.23) | collective-permute-done | bytes 262176 | tf_op jit(solution)/shard_map/ppermute | solution.py:22
  138.5 5.1 %shard_map.87 = (f32[64,2048]{1,0:T(8,128)S(1)}, f32[64,2048]{1,0:T(8,128)S(1)}, f32[64,2048]{1,0:T(8,128)S(1)}, f32[64,2048]{1,0:T(8,128)S(1)}) custom-call(bf16[704,512]{1,0:T(8,128)(2,1)S(1)} %get-tuple-element.29.d_mine.d, bf16[704,512]{1,0:T(8,128)(2,1)S(1)} %get-tuple-element.30.d_other.d, bf16[1056,1536]{1,0:T(8,128)(2,1)S(1)} %get-tuple-element.27.refs_16_.m_most, ...), custom_call_target="tpu_custom_call" | custom-call | tf_op jit(solution)/shard_map/pallas_call | solution.py:66
  143.7 3.3 %collective-permute-start.28 = (bf16[64,2048]{1,0:T(8,128)(2,1)S(1)}, bf16[64,2048]{1,0:T(8,128)(2,1)S(1)}, u32[]{:S(2)}, u32[]{:S(2)}) collective-permute-start(bf16[64,2048]{1,0:T(8,128)(2,1)S(1)} %shard_map.92), channel_id=1, source_target_pairs={{0,14},{2,0},{4,2},{6,4},{8,6},{10,8},{12,10},{14,12},{1,15},{3,1}... | collective-permute-start | bytes 786440 | tf_op jit(solution)/shard_map/ppermute | solution.py:22
  148.9 2.2 %collective-permute-start.36 = (bf16[1056,128]{1,0:T(8,128)(2,1)S(1)}, bf16[1056,128]{1,0:T(8,128)(2,1)S(1)}, u32[]{:S(2)}, u32[]{:S(2)}) collective-permute-start(bf16[1056,128]{1,0:T(8,128)(2,1)S(1)} %get-tuple-element.48), channel_id=1, source_target_pairs={{0,192},{1,49},{16,208},{17,1},{32,224},{33,17},{48,240},{49,33},{... | collective-permute-start | bytes 811016 | tf_op jit(solution)/shard_map/ppermute | solution.py:33
  151.1 2.6 %collective-permute-start.37 = (bf16[1056,128]{1,0:T(8,128)(2,1)S(1)}, bf16[1056,128]{1,0:T(8,128)(2,1)S(1)}, u32[]{:S(2)}, u32[]{:S(2)}) collective-permute-start(bf16[1056,128]{1,0:T(8,128)(2,1)S(1)} %get-tuple-element.49), channel_id=1, source_target_pairs={{0,128},{1,33},{16,144},{17,49},{32,160},{33,1},{48,176},{49,17},{... | collective-permute-start | bytes 811016 | tf_op jit(solution)/shard_map/ppermute | solution.py:33
  153.7 3.3 %collective-permute-start.29 = (bf16[64,2048]{1,0:T(8,128)(2,1)S(1)}, bf16[64,2048]{1,0:T(8,128)(2,1)S(1)}, u32[]{:S(2)}, u32[]{:S(2)}) collective-permute-start(bf16[64,2048]{1,0:T(8,128)(2,1)S(1)} %shard_map.93), channel_id=1, source_target_pairs={{0,14},{2,0},{4,2},{6,4},{8,6},{10,8},{12,10},{14,12},{1,15},{3,1}... | collective-permute-start | bytes 786440 | tf_op jit(solution)/shard_map/ppermute | solution.py:22
  157.1 3.7 %collective-permute-done.29.left = bf16[64,2048]{1,0:T(8,128)(2,1)S(1)} collective-permute-done((bf16[64,2048]{1,0:T(8,128)(2,1)S(1)}, bf16[64,2048]{1,0:T(8,128)(2,1)S(1)}, u32[]{:S(2)}, u32[]{:S(2)}) %collective-permute-start.29) | collective-permute-done | bytes 262176 | tf_op jit(solution)/shard_map/ppermute | solution.py:22
  160.9 3.8 %collective-permute-done.26.right = bf16[64,2048]{1,0:T(8,128)(2,1)S(1)} collective-permute-done((bf16[64,2048]{1,0:T(8,128)(2,1)S(1)}, bf16[64,2048]{1,0:T(8,128)(2,1)S(1)}, u32[]{:S(2)}, u32[]{:S(2)}) %collective-permute-start.26) | collective-permute-done | bytes 262176 | tf_op jit(solution)/shard_map/ppermute | solution.py:22
  (110 shorter events, 46.4 us)
Async XLA Ops:
  1.6 11.4 %collective-permute-start.16 = (bf16[1056,128]{1,0:T(8,128)(2,1)S(1)}, bf16[1056,128]{1,0:T(8,128)(2,1)S(1)}, u32[]{:S(2)}, u32[]{:S(2)}) collective-permute-start(bf16[1056,128]{1,0:T(8,128)(2,1)S(1)} %pad_maximum_fusion), channel_id=1, source_target_pairs={{0,128},{1,33},{16,144},{17,49},{32,160},{33,1},{48,176},{49,17},{... | collective-permute-start | bytes 811016 | tf_op jit(solution)/shard_map/ppermute | solution.py:33
  4.9 8.1 %collective-permute-start.15 = (bf16[1056,128]{1,0:T(8,128)(2,1)S(1)}, bf16[1056,128]{1,0:T(8,128)(2,1)S(1)}, u32[]{:S(2)}, u32[]{:S(2)}) collective-permute-start(bf16[1056,128]{1,0:T(8,128)(2,1)S(1)} %pad_maximum_fusion), channel_id=1, source_target_pairs={{0,64},{1,17},{16,80},{17,33},{32,96},{33,49},{48,112},{49,1},{64,... | collective-permute-start | bytes 811016 | tf_op jit(solution)/shard_map/ppermute | solution.py:33
  13.1 15.2 %collective-permute-start.18 = (bf16[4224,128]{1,0:T(8,128)(2,1)S(1)}, bf16[4224,128]{1,0:T(8,128)(2,1)S(1)}, u32[]{:S(2)}, u32[]{:S(2)}) collective-permute-start(bf16[4224,128]{1,0:T(8,128)(2,1)S(1)} %constant_dynamic-update-slice_fusion.refs_0_), channel_id=1, source_target_pairs={{0,16},{1,65},{16,32},{17,81},{32,48},{33,97},{48,0},{49,113},{64,... | collective-permute-start | bytes 3244040 | tf_op jit(solution)/shard_map/ppermute | solution.py:33
  14.3 15.2 %collective-permute-start.17 = (bf16[4224,128]{1,0:T(8,128)(2,1)S(1)}, bf16[4224,128]{1,0:T(8,128)(2,1)S(1)}, u32[]{:S(2)}, u32[]{:S(2)}) collective-permute-start(bf16[4224,128]{1,0:T(8,128)(2,1)S(1)} %constant_dynamic-update-slice_fusion.refs_0_), channel_id=1, source_target_pairs={{0,48},{1,193},{16,0},{17,209},{32,16},{33,225},{48,32},{49,241},{... | collective-permute-start | bytes 3244040 | tf_op jit(solution)/shard_map/ppermute | solution.py:33
  32.2 59.8 %collective-permute-start.21 = (bf16[1056,1536]{1,0:T(8,128)(2,1)}, bf16[1056,1536]{1,0:T(8,128)(2,1)}, u32[]{:S(2)}, u32[]{:S(2)}) collective-permute-start(bf16[1056,1536]{1,0:T(8,128)(2,1)} %get-tuple-element.28), channel_id=1, source_target_pairs={{0,1},{1,0},{2,3},{3,2},{4,5},{5,4},{6,7},{7,6},{8,9},{9,8},{10,11... | collective-permute-start | bytes 9732104 | tf_op jit(solution)/shard_map/ppermute | solution.py:22
  32.2 10.0 %collective-permute-start.20 = (bf16[2112,128]{1,0:T(8,128)(2,1)S(1)}, bf16[2112,128]{1,0:T(8,128)(2,1)S(1)}, u32[]{:S(2)}, u32[]{:S(2)}) collective-permute-start(bf16[2112,128]{1,0:T(8,128)(2,1)S(1)} %slice.21), channel_id=1, source_target_pairs={{0,16},{1,65},{16,32},{17,81},{32,48},{33,97},{48,0},{49,113},{64,... | collective-permute-start | bytes 1622024 | tf_op jit(solution)/shard_map/ppermute | solution.py:33
  35.3 9.4 %collective-permute-start.19 = (bf16[2112,128]{1,0:T(8,128)(2,1)S(1)}, bf16[2112,128]{1,0:T(8,128)(2,1)S(1)}, u32[]{:S(2)}, u32[]{:S(2)}) collective-permute-start(bf16[2112,128]{1,0:T(8,128)(2,1)S(1)} %slice.20), channel_id=1, source_target_pairs={{0,48},{1,193},{16,0},{17,209},{32,16},{33,225},{48,32},{49,241},{... | collective-permute-start | bytes 1622024 | tf_op jit(solution)/shard_map/ppermute | solution.py:33
  35.4 15.1 %collective-permute-start = (bf16[64,2048]{1,0:T(8,128)(2,1)S(1)}, bf16[64,2048]{1,0:T(8,128)(2,1)S(1)}, u32[]{:S(2)}, u32[]{:S(2)}) collective-permute-start(bf16[64,2048]{1,0:T(8,128)(2,1)S(1)} %copy-done), channel_id=1, source_target_pairs={{0,14},{2,0},{4,2},{6,4},{8,6},{10,8},{12,10},{14,12},{1,15},{3,1}... | collective-permute-start | bytes 786440 | tf_op jit(solution)/shard_map/ppermute | solution.py:22
  40.3 10.3 %collective-permute-start.1 = (bf16[64,2048]{1,0:T(8,128)(2,1)S(1)}, bf16[64,2048]{1,0:T(8,128)(2,1)S(1)}, u32[]{:S(2)}, u32[]{:S(2)}) collective-permute-start(bf16[64,2048]{1,0:T(8,128)(2,1)S(1)} %copy-done), channel_id=1, source_target_pairs={{0,2},{2,4},{4,6},{6,8},{8,10},{10,12},{12,14},{14,0},{1,3},{3,5},... | collective-permute-start | bytes 786440 | tf_op jit(solution)/shard_map/ppermute | solution.py:22
  46.0 46.0 %collective-permute-start.22 = (bf16[1056,512]{1,0:T(8,128)(2,1)}, bf16[1056,512]{1,0:T(8,128)(2,1)}, u32[]{:S(2)}, u32[]{:S(2)}) collective-permute-start(bf16[1056,512]{1,0:T(8,128)(2,1)} %shard_map.85.refs_17_.m_last), channel_id=1, source_target_pairs={{0,1},{1,0},{2,3},{3,2},{4,5},{5,4},{6,7},{7,6},{8,9},{9,8},{10,11... | collective-permute-start | bytes 3244040 | tf_op jit(solution)/shard_map/ppermute | solution.py:22
  46.0 11.2 %collective-permute-start.7 = (bf16[64,2048]{1,0:T(8,128)(2,1)S(1)}, bf16[64,2048]{1,0:T(8,128)(2,1)S(1)}, u32[]{:S(2)}, u32[]{:S(2)}) collective-permute-start(bf16[64,2048]{1,0:T(8,128)(2,1)S(1)} %copy-done.1), channel_id=1, source_target_pairs={{0,14},{2,0},{4,2},{6,4},{8,6},{10,8},{12,10},{14,12},{1,15},{3,1}... | collective-permute-start | bytes 786440 | tf_op jit(solution)/shard_map/ppermute | solution.py:22
  50.5 9.6 %collective-permute-start.8 = (bf16[64,2048]{1,0:T(8,128)(2,1)S(1)}, bf16[64,2048]{1,0:T(8,128)(2,1)S(1)}, u32[]{:S(2)}, u32[]{:S(2)}) collective-permute-start(bf16[64,2048]{1,0:T(8,128)(2,1)S(1)} %copy-done.1), channel_id=1, source_target_pairs={{0,2},{2,4},{4,6},{6,8},{8,10},{10,12},{12,14},{14,0},{1,3},{3,5},... | collective-permute-start | bytes 786440 | tf_op jit(solution)/shard_map/ppermute | solution.py:22
  50.6 12.2 %collective-permute-start.2 = (bf16[64,2048]{1,0:T(8,128)(2,1)S(1)}, bf16[64,2048]{1,0:T(8,128)(2,1)S(1)}, u32[]{:S(2)}, u32[]{:S(2)}) collective-permute-start(bf16[64,2048]{1,0:T(8,128)(2,1)S(1)} %collective-permute-done.refs_1_), channel_id=1, source_target_pairs={{0,14},{2,0},{4,2},{6,4},{8,6},{10,8},{12,10},{14,12},{1,15},{3,1}... | collective-permute-start | bytes 786440 | tf_op jit(solution)/shard_map/ppermute | solution.py:22
  57.2 9.3 %collective-permute-start.3 = (bf16[64,2048]{1,0:T(8,128)(2,1)S(1)}, bf16[64,2048]{1,0:T(8,128)(2,1)S(1)}, u32[]{:S(2)}, u32[]{:S(2)}) collective-permute-start(bf16[64,2048]{1,0:T(8,128)(2,1)S(1)} %collective-permute-done.1.refs_2_), channel_id=1, source_target_pairs={{0,2},{2,4},{4,6},{6,8},{8,10},{10,12},{12,14},{14,0},{1,3},{3,5},... | collective-permute-start | bytes 786440 | tf_op jit(solution)/shard_map/ppermute | solution.py:22
  60.2 8.8 %collective-permute-start.9 = (bf16[64,2048]{1,0:T(8,128)(2,1)S(1)}, bf16[64,2048]{1,0:T(8,128)(2,1)}, u32[]{:S(2)}, u32[]{:S(2)}) collective-permute-start(bf16[64,2048]{1,0:T(8,128)(2,1)S(1)} %collective-permute-done.7.refs_9_), channel_id=1, source_target_pairs={{0,14},{2,0},{4,2},{6,4},{8,6},{10,8},{12,10},{14,12},{1,15},{3,1}... | collective-permute-start | bytes 786440 | tf_op jit(solution)/shard_map/ppermute | solution.py:22
  62.9 9.3 %collective-permute-start.10 = (bf16[64,2048]{1,0:T(8,128)(2,1)S(1)}, bf16[64,2048]{1,0:T(8,128)(2,1)S(1)}, u32[]{:S(2)}, u32[]{:S(2)}) collective-permute-start(bf16[64,2048]{1,0:T(8,128)(2,1)S(1)} %collective-permute-done.8.refs_10_), channel_id=1, source_target_pairs={{0,2},{2,4},{4,6},{6,8},{8,10},{10,12},{12,14},{14,0},{1,3},{3,5},... | collective-permute-start | bytes 786440 | tf_op jit(solution)/shard_map/ppermute | solution.py:22
  69.0 10.4 %collective-permute-start.5 = (bf16[64,2048]{1,0:T(8,128)(2,1)S(1)}, bf16[64,2048]{1,0:T(8,128)(2,1)S(1)}, u32[]{:S(2)}, u32[]{:S(2)}) collective-permute-start(bf16[64,2048]{1,0:T(8,128)(2,1)S(1)} %collective-permute-done.3.refs_4_), channel_id=1, source_target_pairs={{0,2},{2,4},{4,6},{6,8},{8,10},{10,12},{12,14},{14,0},{1,3},{3,5},... | collective-permute-start | bytes 786440 | tf_op jit(solution)/shard_map/ppermute | solution.py:22
  72.2 11.4 %collective-permute-start.12 = (bf16[64,2048]{1,0:T(8,128)(2,1)S(1)}, bf16[64,2048]{1,0:T(8,128)(2,1)}, u32[]{:S(2)}, u32[]{:S(2)}) collective-permute-start(bf16[64,2048]{1,0:T(8,128)(2,1)S(1)} %collective-permute-done.10.refs_12_), channel_id=1, source_target_pairs={{0,2},{2,4},{4,6},{6,8},{8,10},{10,12},{12,14},{14,0},{1,3},{3,5},... | collective-permute-start | bytes 786440 | tf_op jit(solution)/shard_map/ppermute | solution.py:22
  73.6 10.8 %collective-permute-start.11 = (bf16[64,2048]{1,0:T(8,128)(2,1)}, bf16[64,2048]{1,0:T(8,128)(2,1)}, u32[]{:S(2)}, u32[]{:S(2)}) collective-permute-start(bf16[64,2048]{1,0:T(8,128)(2,1)} %collective-permute-done.9.refs_11_), channel_id=1, source_target_pairs={{0,14},{2,0},{4,2},{6,4},{8,6},{10,8},{12,10},{14,12},{1,15},{3,1}... | collective-permute-start | bytes 786440 | tf_op jit(solution)/shard_map/ppermute | solution.py:22
  83.6 8.3 %collective-permute-start.13 = (bf16[64,2048]{1,0:T(8,128)(2,1)}, bf16[64,2048]{1,0:T(8,128)(2,1)}, u32[]{:S(2)}, u32[]{:S(2)}) collective-permute-start(bf16[64,2048]{1,0:T(8,128)(2,1)} %collective-permute-done.12.refs_14_), channel_id=1, source_target_pairs={{0,2},{2,4},{4,6},{6,8},{8,10},{10,12},{12,14},{14,0},{1,3},{3,5},... | collective-permute-start | bytes 786440 | tf_op jit(solution)/shard_map/ppermute | solution.py:22
  118.0 29.1 %collective-permute-start.31 = (bf16[1056,512]{1,0:T(8,128)(2,1)S(1)}, bf16[1056,512]{1,0:T(8,128)(2,1)S(1)}, u32[]{:S(2)}, u32[]{:S(2)}) collective-permute-start(bf16[1056,512]{1,0:T(8,128)(2,1)S(1)} %get-tuple-element.43), channel_id=1, source_target_pairs={{0,16},{1,65},{16,32},{17,81},{32,48},{33,97},{48,0},{49,113},{64,... | collective-permute-start | bytes 3244040 | tf_op jit(solution)/shard_map/ppermute | solution.py:33
  121.1 26.1 %collective-permute-start.33 = (bf16[1056,512]{1,0:T(8,128)(2,1)S(1)}, bf16[1056,512]{1,0:T(8,128)(2,1)S(1)}, u32[]{:S(2)}, u32[]{:S(2)}) collective-permute-start(bf16[1056,512]{1,0:T(8,128)(2,1)S(1)} %get-tuple-element.44), channel_id=1, source_target_pairs={{0,48},{1,193},{16,0},{17,209},{32,16},{33,225},{48,32},{49,241},{... | collective-permute-start | bytes 3244040 | tf_op jit(solution)/shard_map/ppermute | solution.py:33
  121.7 25.4 %collective-permute-start.34 = (bf16[1056,512]{1,0:T(8,128)(2,1)S(1)}, bf16[1056,512]{1,0:T(8,128)(2,1)S(1)}, u32[]{:S(2)}, u32[]{:S(2)}) collective-permute-start(bf16[1056,512]{1,0:T(8,128)(2,1)S(1)} %get-tuple-element.45), channel_id=1, source_target_pairs={{0,32},{1,129},{16,48},{17,145},{32,0},{33,161},{48,16},{49,177},{... | collective-permute-start | bytes 3244040 | tf_op jit(solution)/shard_map/ppermute | solution.py:33
  129.3 9.1 %collective-permute-start.23 = (bf16[64,2048]{1,0:T(8,128)(2,1)S(1)}, bf16[64,2048]{1,0:T(8,128)(2,1)S(1)}, u32[]{:S(2)}, u32[]{:S(2)}) collective-permute-start(bf16[64,2048]{1,0:T(8,128)(2,1)S(1)} %get-tuple-element.35), channel_id=1, source_target_pairs={{0,2},{2,4},{4,6},{6,8},{8,10},{10,12},{12,14},{14,0},{1,3},{3,5},... | collective-permute-start | bytes 786440 | tf_op jit(solution)/shard_map/ppermute | solution.py:22
  129.4 14.2 %collective-permute-start.27 = (bf16[64,2048]{1,0:T(8,128)(2,1)S(1)}, bf16[64,2048]{1,0:T(8,128)(2,1)S(1)}, u32[]{:S(2)}, u32[]{:S(2)}) collective-permute-start(bf16[64,2048]{1,0:T(8,128)(2,1)S(1)} %get-tuple-element.38), channel_id=1, source_target_pairs={{0,14},{2,0},{4,2},{6,4},{8,6},{10,8},{12,10},{14,12},{1,15},{3,1}... | collective-permute-start | bytes 786440 | tf_op jit(solution)/shard_map/ppermute | solution.py:22
  138.4 8.6 %collective-permute-start.24 = (bf16[64,2048]{1,0:T(8,128)(2,1)S(1)}, bf16[64,2048]{1,0:T(8,128)(2,1)S(1)}, u32[]{:S(2)}, u32[]{:S(2)}) collective-permute-start(bf16[64,2048]{1,0:T(8,128)(2,1)S(1)} %shard_map.89), channel_id=1, source_target_pairs={{0,2},{2,4},{4,6},{6,8},{8,10},{10,12},{12,14},{14,0},{1,3},{3,5},... | collective-permute-start | bytes 786440 | tf_op jit(solution)/shard_map/ppermute | solution.py:22
  143.7 10.0 %collective-permute-start.28 = (bf16[64,2048]{1,0:T(8,128)(2,1)S(1)}, bf16[64,2048]{1,0:T(8,128)(2,1)S(1)}, u32[]{:S(2)}, u32[]{:S(2)}) collective-permute-start(bf16[64,2048]{1,0:T(8,128)(2,1)S(1)} %shard_map.92), channel_id=1, source_target_pairs={{0,14},{2,0},{4,2},{6,4},{8,6},{10,8},{12,10},{14,12},{1,15},{3,1}... | collective-permute-start | bytes 786440 | tf_op jit(solution)/shard_map/ppermute | solution.py:22
  147.0 10.0 %collective-permute-start.25 = (bf16[64,2048]{1,0:T(8,128)(2,1)S(1)}, bf16[64,2048]{1,0:T(8,128)(2,1)S(1)}, u32[]{:S(2)}, u32[]{:S(2)}) collective-permute-start(bf16[64,2048]{1,0:T(8,128)(2,1)S(1)} %shard_map.90), channel_id=1, source_target_pairs={{0,2},{2,4},{4,6},{6,8},{8,10},{10,12},{12,14},{14,0},{1,3},{3,5},... | collective-permute-start | bytes 786440 | tf_op jit(solution)/shard_map/ppermute | solution.py:22
  147.8 18.3 %collective-permute-start.35 = (bf16[1056,128]{1,0:T(8,128)(2,1)S(1)}, bf16[1056,128]{1,0:T(8,128)(2,1)S(1)}, u32[]{:S(2)}, u32[]{:S(2)}) collective-permute-start(bf16[1056,128]{1,0:T(8,128)(2,1)S(1)} %get-tuple-element.47), channel_id=1, source_target_pairs={{0,64},{1,17},{16,80},{17,33},{32,96},{33,49},{48,112},{49,1},{64,... | collective-permute-start | bytes 811016 | tf_op jit(solution)/shard_map/ppermute | solution.py:33
  148.9 17.2 %collective-permute-start.36 = (bf16[1056,128]{1,0:T(8,128)(2,1)S(1)}, bf16[1056,128]{1,0:T(8,128)(2,1)S(1)}, u32[]{:S(2)}, u32[]{:S(2)}) collective-permute-start(bf16[1056,128]{1,0:T(8,128)(2,1)S(1)} %get-tuple-element.48), channel_id=1, source_target_pairs={{0,192},{1,49},{16,208},{17,1},{32,224},{33,17},{48,240},{49,33},{... | collective-permute-start | bytes 811016 | tf_op jit(solution)/shard_map/ppermute | solution.py:33
  151.1 15.0 %collective-permute-start.37 = (bf16[1056,128]{1,0:T(8,128)(2,1)S(1)}, bf16[1056,128]{1,0:T(8,128)(2,1)S(1)}, u32[]{:S(2)}, u32[]{:S(2)}) collective-permute-start(bf16[1056,128]{1,0:T(8,128)(2,1)S(1)} %get-tuple-element.49), channel_id=1, source_target_pairs={{0,128},{1,33},{16,144},{17,49},{32,160},{33,1},{48,176},{49,17},{... | collective-permute-start | bytes 811016 | tf_op jit(solution)/shard_map/ppermute | solution.py:33
  157.1 7.7 %collective-permute-start.26 = (bf16[64,2048]{1,0:T(8,128)(2,1)S(1)}, bf16[64,2048]{1,0:T(8,128)(2,1)S(1)}, u32[]{:S(2)}, u32[]{:S(2)}) collective-permute-start(bf16[64,2048]{1,0:T(8,128)(2,1)S(1)} %shard_map.91), channel_id=1, source_target_pairs={{0,2},{2,4},{4,6},{6,8},{8,10},{10,12},{12,14},{14,0},{1,3},{3,5},... | collective-permute-start | bytes 786440 | tf_op jit(solution)/shard_map/ppermute | solution.py:22
  (25 other events, 68.2 us)
